TPU v7x, 32 devices: a whole 2x2x4 slice. The times are simulated.
32 devices in a mesh: sp: 16 (over z, y, x), tp: 2 (over core).
Axes of the slice: x: 2, y: 2, z: 4, core: 2. Of those that a mesh axis runs over, the one named last changes fastest.
Arguments:
- stream: bfloat16 [4096, 2048], P(('sp', 'tp')), may hold values from -6 to 6
- queries: bfloat16 [4096, 1024], P('sp', 'tp'), may hold values from -6 to 6
- keys_in: bfloat16 [4096, 1024], P('sp', 'tp'), may hold values from -6 to 6
- values_in: bfloat16 [4096, 1024], P('sp', 'tp'), may hold values from -6 to 6
- gate_in: bfloat16 [4096, 1024], P('sp', 'tp'), may hold values from -6 to 6
- log_decay: float32 [4096, 8], P('sp', 'tp'), may hold values from -0.8 to 0
- head_gain: bfloat16 [1024], P('tp'), may hold values from 0.099609375 to 1.8984375
- out_weight: bfloat16 [1024, 2048], P('tp'), may hold values from -0.1875 to 0.1875
- norm_gain: bfloat16 [2048], replicated, may hold values from 0.099609375 to 1.8984375
- gate_weight: bfloat16 [2048, 5632], P('sp', 'tp'), may hold values from -0.125 to 0.125
- up_weight: bfloat16 [2048, 5632], P('sp', 'tp'), may hold values from -0.125 to 0.125
- down_weight: bfloat16 [5632, 2048], P('tp', 'sp'), may hold values from -0.078125 to 0.078125
Outputs:
- result: bfloat16 [4096, 2048], P(('sp', 'tp'))
All inputs are finite; a program needn't handle non-finite values.
Results may differ from a plain program's by a relative error of at most 0.02.
Values may be sent and summed in bfloat16 or wider, within the bound.
A program may use at most 128 MiB of HBM per device.

v0:
```python
import jax
import jax.numpy as jnp
from jax import lax
from jax.sharding import PartitionSpec as P

BLOCK = 128
epsilon = 1e-06
highest = lax.Precision.HIGHEST


def carried_in(value, axis, combine, identity):
    length, here = (lax.axis_size(axis), lax.axis_index(axis))
    everything = jax.tree.map(
        lambda part, kind: lax.all_gather(part.astype(kind), axis),
        value,
        (jnp.bfloat16, jnp.bfloat16),
    )
    start = jax.tree.map(
        lambda part, zero: jnp.broadcast_to(jnp.asarray(zero, part.dtype), part.shape),
        value,
        identity,
    )

    def turn(k, before):
        reached = k < here
        new = combine(
            before, jax.tree.map(lambda part, own: part[k].astype(own.dtype), everything, value)
        )
        return jax.tree.map(lambda a, b: jnp.where(reached, a, b), new, before)

    return lax.fori_loop(0, length, turn, start)


def block_pass(state, block_inputs):
    query_block, key_block, value_block, decay_block = block_inputs
    head_dim = query_block.shape[-1]
    key_scale = head_dim ** (-0.5)
    running = jnp.cumsum(decay_block, axis=0)
    scores = (
        jnp.einsum("ihd,jhd->hij", query_block, key_block, preferred_element_type=jnp.float32)
        * key_scale
    )
    offsets = jnp.arange(decay_block.shape[0])
    causal = offsets[:, None] >= offsets[None, :]
    log_gap = running.T[:, :, None] - running.T[:, None, :]
    decay_table = jnp.where(causal[None], jnp.exp(jnp.minimum(log_gap, 0.0)), 0.0)
    value_wide = value_block.astype(jnp.float32)
    within = jnp.einsum("hij,jhe->ihe", scores * decay_table, value_wide, precision=highest)
    query_wide = query_block.astype(jnp.float32) * jnp.exp(running)[:, :, None]
    carried = jnp.einsum("ihd,hde->ihe", query_wide, state, precision=highest)
    block_total = running[-1]
    key_wide = (
        key_block.astype(jnp.float32) * key_scale * jnp.exp(block_total[None] - running)[:, :, None]
    )
    state = jnp.exp(block_total)[:, None, None] * state + jnp.einsum(
        "jhd,jhe->hde", key_wide, value_wide, precision=highest
    )
    return (state, within + carried)


def chain_combine(earlier_pair, later_pair):
    return (
        earlier_pair[0] * later_pair[0],
        later_pair[0][:, None, None] * earlier_pair[1] + later_pair[1],
    )


def local(
    stream,
    queries,
    keys_in,
    values_in,
    gate_in,
    log_decay,
    head_gain,
    out_weight,
    norm_gain,
    gate_weight,
    up_weight,
    down_weight,
):
    gate_full, up_full = (
        lax.all_gather(gate_weight, "sp", axis=0, tiled=True),
        lax.all_gather(up_weight, "sp", axis=0, tiled=True),
    )
    down_full = lax.all_gather(down_weight, "sp", axis=1, tiled=True)
    row_count, heads_here = log_decay.shape
    head_dim = queries.shape[1] // heads_here
    block_count = row_count // BLOCK
    block_shape = (block_count, BLOCK, heads_here, head_dim)
    block_inputs = (
        queries.reshape(block_shape),
        keys_in.reshape(block_shape),
        values_in.reshape(block_shape),
        log_decay.reshape(block_count, BLOCK, heads_here),
    )
    start_state = jnp.zeros((heads_here, head_dim, head_dim), jnp.float32)
    final_state, within = lax.scan(block_pass, start_state, block_inputs)
    within = within.reshape(row_count, heads_here, head_dim)
    running = jnp.cumsum(log_decay, axis=0)
    device_total = running[-1]
    scanned = carried_in(
        (jnp.exp(device_total), final_state),
        "sp",
        chain_combine,
        (jnp.ones_like(device_total), jnp.zeros_like(final_state)),
    )
    incoming = scanned[1]
    query_wide = (
        queries.reshape(row_count, heads_here, head_dim).astype(jnp.float32)
        * jnp.exp(running)[:, :, None]
    )
    retained = within + jnp.einsum("ihd,hde->ihe", query_wide, incoming, precision=highest)
    center = jnp.mean(retained, axis=-1, keepdims=True)
    spread = jnp.mean(jnp.square(retained - center), axis=-1, keepdims=True)
    normed_heads = (
        (retained - center)
        * lax.rsqrt(spread + epsilon)
        * head_gain.astype(jnp.float32).reshape(heads_here, head_dim)
    )
    mixed = (
        jax.nn.silu(gate_in.astype(jnp.float32))
        * normed_heads.reshape(row_count, heads_here * head_dim)
    ).astype(jnp.bfloat16)
    attended = lax.psum_scatter(
        jnp.dot(mixed, out_weight, preferred_element_type=jnp.float32).astype(jnp.bfloat16),
        "tp",
        scatter_dimension=0,
        tiled=True,
    ).astype(jnp.float32)
    residual = stream.astype(jnp.float32) + attended
    normed = (
        residual
        * lax.rsqrt(jnp.mean(residual * residual, axis=-1, keepdims=True) + epsilon)
        * norm_gain.astype(jnp.float32)
    ).astype(jnp.bfloat16)
    whole_rows = lax.all_gather(normed, "tp", axis=0, tiled=True)
    gate_sum = jnp.dot(whole_rows, gate_full, preferred_element_type=jnp.float32)
    up_sum = jnp.dot(whole_rows, up_full, preferred_element_type=jnp.float32)
    hidden = (jax.nn.silu(gate_sum) * up_sum).astype(jnp.bfloat16)
    down_terms = jnp.dot(hidden, down_full, preferred_element_type=jnp.float32)
    mixer_out = lax.psum_scatter(
        down_terms.astype(jnp.bfloat16), "tp", scatter_dimension=0, tiled=True
    ).astype(jnp.float32)
    return (residual + mixer_out).astype(jnp.bfloat16)


def solution(mesh):
    return jax.shard_map(
        local,
        mesh=mesh,
        in_specs=(
            P(("sp", "tp"), None),
            P("sp", "tp"),
            P("sp", "tp"),
            P("sp", "tp"),
            P("sp", "tp"),
            P("sp", "tp"),
            P("tp"),
            P("tp", None),
            P(),
            P("sp", "tp"),
            P("sp", "tp"),
            P("tp", "sp"),
        ),
        out_specs=P(("sp", "tp"), None),
        check_vma=False,
    )
```

profile of v0, /device:TPU:0, one launch (start us, length us, event | category | flops | bytes accessed | tf_op | source)
XLA Modules:
  0.0 643.5 jit_solution(10230276023747323382)
XLA Ops:
  6.5 1.9 reshape.105
  8.4 1.7 reshape.106
  10.1 1.7 reshape.107
  12.7 24.1 %while.27 = (s32[]{:T(128)}, f32[4,128,128]{2,1,0:T(8,128)S(1)}, f32[2,128,4,128]{1,0,3,2:T(2,128)}, f32[2,128,4]{2,1,0:T(8,128)S(1)}, bf16[2,128,4,128]{3,2,1,0...) while((s32[]{:T(128)}, f32[4,128,128]{2,1,0:T(8,128)S(1)}, ...), condition=%wide.region_2.3_spmd.clone, body=%wide.region_0.2_spmd.clone.sunk | while | flops 319767040 | bytes 4260068 | solution.py:98
  12.7 1.1 constant_dynamic-slice_fusion.6
  16.5 7.7 %dynamic_update_slice.6 = f32[2,128,4,128]{1,0,3,2:T(2,128)} dynamic-update-slice(f32[2,128,4,128]{1,0,3,2:T(2,128)} %get-tuple-element.359, f32[1,128,4,128]{1,0,3,2:T(1,128)S(1)} %bitcast.115, s32[]{:T(128)} %get-tuple-element.357, s32[]{:T(128)} %constant.67.clone.1..sunk, s32[]{:T(128)} %constant.67.clone.1..sunk, s32[]{:T(128)} %constant.67.clone.1..sunk) | dynamic-update-slice | bytes 524292 | tf_op jit(solution)/shard_map/while/body/jit(dynamic_update_index_in_dim)/dynamic_update_slice | solution.py:98
  28.5 7.7 %dynamic_update_slice.6 = f32[2,128,4,128]{1,0,3,2:T(2,128)} dynamic-update-slice(f32[2,128,4,128]{1,0,3,2:T(2,128)} %get-tuple-element.359, f32[1,128,4,128]{1,0,3,2:T(1,128)S(1)} %bitcast.115, s32[]{:T(128)} %get-tuple-element.357, s32[]{:T(128)} %constant.67.clone.1..sunk, s32[]{:T(128)} %constant.67.clone.1..sunk, s32[]{:T(128)} %constant.67.clone.1..sunk) | dynamic-update-slice | bytes 524292 | tf_op jit(solution)/shard_map/while/body/jit(dynamic_update_index_in_dim)/dynamic_update_slice | solution.py:98
  37.5 1.2 reduce-window.6
  39.3 42.5 %all-gather.1 = bf16[16,1,4]{2,1,0:T(2,128)(2,1)S(1)} all-gather(bf16[1,1,4]{2,1,0:T(2,128)(2,1)S(1)} %bitcast.124), channel_id=1, replica_groups=mesh['sp'=16,'tp'=2] {'sp'}, dimensions={0}, use_global_device_ids=true | all-gather | bytes 136 | tf_op jit(solution)/shard_map/all_gather | solution.py:14
  82.0 1.5 reshape.108
  83.5 17.2 %all-gather.16.cloned.1.call-done = bf16[64,128,128]{2,1,0:T(8,128)(2,1)} async-done(((bf16[4,128,128]{2,1,0:T(8,128)(2,1)}), bf16[64,128,128]{2,1,0:T(8,128)(2,1)}) %all-gather.16.cloned.1.call-update) | async-done | bytes 2097168 | tf_op jit(solution)/shard_map/all_gather | solution.py:14
  100.7 16.8 %while.28 = (s32[]{:T(128)}, f32[4,128,128]{2,1,0:T(8,128)S(1)}, s32[]{:T(128)}, bf16[16,4]{1,0:T(8,128)(2,1)S(1)}, bf16[16,4,128,128]{3,2,1,0:T(8,128)(2,1)}, /*index=5*/s32[]{:T(128)}, s32[]{:T(128)}) while((s32[]{:T(128)}, f32[4,128,128]{2,1,0:T(8,128)S(1)}, s32[]{:T(128)}, bf16[16,4]{1,0:T(8,128)(2,1)S(1)}, ...), condition=%wide.region_6.7_spmd.clone, body=%wide.region_5.6_spmd.clone.sunk | while | flops 327688 | bytes 655505 | solution.py:31
  118.8 1.7 convolution_convert_fusion.1
  120.6 7.3 %reduce-scatter.3.cloned.1.call-done = bf16[128,2048]{1,0:T(8,128)(2,1)} async-done(((bf16[256,2048]{1,0:T(8,128)(2,1)}), bf16[128,2048]{1,0:T(8,128)(2,1)}) %reduce-scatter.3.cloned.1.call-update) | async-done | bytes 524304 | tf_op jit(solution)/shard_map/reduce_scatter | solution.py:125
  127.9 1.3 multiply_reduce_fusion
  129.2 2.0 multiply_convert_fusion
  133.3 8.4 %all-gather.8.cloned.1.call-done = bf16[256,2048]{1,0:T(8,128)(2,1)} async-done(((bf16[128,2048]{1,0:T(8,128)(2,1)}), bf16[256,2048]{1,0:T(8,128)(2,1)}) %all-gather.8.cloned.1.call-update) | async-done | bytes 1048592 | tf_op jit(solution)/shard_map/all_gather | solution.py:137
  141.7 145.2 %all-gather.10.cloned.1.call-done = bf16[2048,2816]{1,0:T(8,128)(2,1)} async-done(((bf16[128,2816]{1,0:T(8,128)(2,1)}), bf16[2048,2816]{1,0:T(8,128)(2,1)}) %all-gather.10.cloned.1.call-update) | async-done | bytes 11534352 | tf_op jit(solution)/shard_map/all_gather | solution.py:83
  286.9 9.4 %fusion.32 = f32[256,2816]{1,0:T(8,128)} fusion(bf16[256,2048]{1,0:T(8,128)(2,1)} %all-gather.8.cloned.1.call-done, bf16[2048,2816]{1,0:T(8,128)(2,1)} %all-gather.10.cloned.1.call-done), kind=kOutput, calls=%fused_computation.68 | convolution fusion | flops 2952790016 | bytes 15466496 | tf_op jit(solution)/shard_map/dot_general | solution.py:138
  296.3 132.8 %all-gather.12.cloned.1.call-done = bf16[2048,2816]{1,0:T(8,128)(2,1)} async-done(((bf16[128,2816]{1,0:T(8,128)(2,1)}), bf16[2048,2816]{1,0:T(8,128)(2,1)}) %all-gather.12.cloned.1.call-update) | async-done | bytes 11534352 | tf_op jit(solution)/shard_map/all_gather | solution.py:84
  429.2 182.8 %all-gather.14.cloned.1.call-done = bf16[2816,2048]{1,0:T(8,128)(2,1)} async-done(((bf16[2816,128]{1,0:T(8,128)(2,1)}), bf16[2816,2048]{1,0:T(8,128)(2,1)}) %all-gather.14.cloned.1.call-update) | async-done | bytes 11534352 | tf_op jit(solution)/shard_map/all_gather | solution.py:86
  612.0 15.9 %convolution_convert_fusion = bf16[256,2048]{1,0:T(8,128)(2,1)} fusion(bf16[2816,2048]{1,0:T(8,128)(2,1)} %all-gather.14.cloned.1.call-done, bf16[256,2048]{1,0:T(8,128)(2,1)} %all-gather.8.cloned.1.call-done, bf16[2048,2816]{1,0:T(8,128)(2,1)} %all-gather.12.cloned.1.call-done, f32[256,2816]{1,0:T(8,128)} %fusion.32), kind=kOutput, calls=%fused_computation.32 | convolution fusion | flops 5910429696 | bytes 28049408 | tf_op jit(solution)/shard_map/dot_general | solution.py:141
  627.9 6.7 %reduce-scatter.5.cloned.1.call-done = bf16[128,2048]{1,0:T(8,128)(2,1)} async-done(((bf16[256,2048]{1,0:T(8,128)(2,1)}), bf16[128,2048]{1,0:T(8,128)(2,1)}) %reduce-scatter.5.cloned.1.call-update) | async-done | bytes 524304 | tf_op jit(solution)/shard_map/reduce_scatter | solution.py:142
  634.6 2.1 add_convert_fusion
  (117 shorter events, 29.5 us)
Async XLA Ops:
  6.5 112.2 %copy-start = (bf16[512,2048]{1,0:T(8,128)(2,1)S(1)}, bf16[512,2048]{1,0:T(8,128)(2,1)}, u32[]{:S(2)}) copy-start(bf16[512,2048]{1,0:T(8,128)(2,1)} %param.23) | copy-start | bytes 6291460
  6.5 94.1 %all-gather.16.cloned.1.call-start = ((), (), s32[]{:S(2)}) async-start(), calls=%async_computation.8 | async-start | bytes 2228224 | tf_op jit(solution)/shard_map/all_gather | solution.py:14
  12.6 24.9 %copy-start.4 = (f32[256,4]{0,1:T(4,128)S(1)}, f32[256,4]{0,1:T(4,128)}, u32[]{:S(2)}) copy-start(f32[256,4]{0,1:T(4,128)} %param.21) | copy-start | bytes 12292
  12.7 70.8 %copy-start.6 = (bf16[512]{0:T(512)(128)(2,1)S(1)}, bf16[512]{0:T(512)(128)(2,1)}, u32[]{:S(2)}) copy-start(bf16[512]{0:T(512)(128)(2,1)} %param.22) | copy-start | bytes 3076
  36.7 80.8 %copy-start.3 = (bf16[256,512]{1,0:T(8,128)(2,1)S(1)}, bf16[256,512]{1,0:T(8,128)(2,1)}, u32[]{:S(2)}) copy-start(bf16[256,512]{1,0:T(8,128)(2,1)} %param.17) | copy-start | bytes 786436
  37.4 90.5 %reduce-scatter.3.cloned.1.call-start = ((), (), s32[]{:S(2)}) async-start(), calls=%async_computation.2 | async-start | bytes 1572864 | tf_op jit(solution)/shard_map/reduce_scatter | solution.py:125
  117.5 1.3 copy-start.7
  118.8 1.8 copy-start.5
  118.8 9.1 %copy-start.1 = (bf16[128,2048]{1,0:T(8,128)(2,1)S(1)}, bf16[128,2048]{1,0:T(8,128)(2,1)}, u32[]{:S(2)}) copy-start(bf16[128,2048]{1,0:T(8,128)(2,1)} %param.16) | copy-start | bytes 1572868
  120.6 21.1 %all-gather.8.cloned.1.call-start = ((), (), s32[]{:S(2)}) async-start(), calls=%async_computation.3 | async-start | bytes 1572864 | tf_op jit(solution)/shard_map/all_gather | solution.py:137
  131.3 155.6 %all-gather.10.cloned.1.call-start = ((), (), s32[]{:S(2)}) async-start(), calls=%async_computation.4 | async-start | bytes 12255232 | tf_op jit(solution)/shard_map/all_gather | solution.py:83
  131.9 297.3 %all-gather.12.cloned.1.call-start = ((), (), s32[]{:S(2)}) async-start(), calls=%async_computation.5 | async-start | bytes 12255232 | tf_op jit(solution)/shard_map/all_gather | solution.py:84
  132.5 479.5 %all-gather.14.cloned.1.call-start = ((), (), s32[]{:S(2)}) async-start(), calls=%async_computation.6 | async-start | bytes 12255232 | tf_op jit(solution)/shard_map/all_gather | solution.py:86
  133.0 501.6 %reduce-scatter.5.cloned.1.call-start = ((), (), s32[]{:S(2)}) async-start(), calls=%async_computation.7 | async-start | bytes 1572864 | tf_op jit(solution)/shard_map/reduce_scatter | solution.py:142
  296.3 338.3 %copy-start.2 = (bf16[128,2048]{1,0:T(8,128)(2,1)S(1)}, bf16[128,2048]{1,0:T(8,128)(2,1)}, u32[]{:S(2)}) copy-start(bf16[128,2048]{1,0:T(8,128)(2,1)} %reduce-scatter.3.cloned.1.call-done) | copy-start | bytes 1572868
Sparse Core Ops, SparseCore 0:
  37.6 63.0 all-gather.15
  120.7 7.1 reduce-scatter.2
  131.4 10.2 all-gather.7
  144.3 142.5 all-gather.9
  289.5 139.5 all-gather.11
  431.7 180.2 all-gather.13
  628.0 6.5 reduce-scatter.4
where the time goes:
time: 645 us; the launch traced here: 644 us
  waiting for transfers between devices  502 us (78%)
  blocking collectives  42.5 us (7%)
  matrix products  31.5 us (5%)
  local copies, waits for them, and re-layouts  28.1 us (4%)
  other arithmetic  24.6 us (4%)
  between operations  13.7 us (2%)
    all_gather x1, waiting for transfers between devices, local(): down_full = lax.all_gather(down_weight, 'sp', axis=1, tiled=True)  183 us
    all_gather x1, waiting for transfers between devices, local(): lax.all_gather(gate_weight, 'sp', axis=0, tiled=True)  145 us
    all_gather x1, waiting for transfers between devices, local(): lax.all_gather(up_weight, 'sp', axis=0, tiled=True)  133 us
    all_gather x1, blocking collectives, carried_in(): lax.all_gather(part.astype(kind), axis)  42.5 us
    all_gather x1, waiting for transfers between devices, carried_in(): lax.all_gather(part.astype(kind), axis)  17.2 us
    select_n x16, other arithmetic, turn(): return jax.tree.map(lambda a, b: jnp.where(reached, a, b), new, before)  16.2 us
    dot_general x1, matrix products, local(): down_terms = jnp.dot(hidden, down_full, preferred_element_type=jnp.float32)  15.9 us
    dynamic_update_slice x2, local copies, waits for them, and re-layouts, local(): final_state, within = lax.scan(block_pass, start_state, block_inputs)  15.3 us
  transfers between devices with their start and end apart: 7, of which 7 were waited for; matrix products, arithmetic and copies ran while one was open for 2% of the time, Pallas kernels for 0%

commit v1 on v0

--- a/solution.py
+++ b/solution.py
@@ -83,7 +83,7 @@
         lax.all_gather(gate_weight, "sp", axis=0, tiled=True),
         lax.all_gather(up_weight, "sp", axis=0, tiled=True),
     )
-    down_full = lax.all_gather(down_weight, "sp", axis=1, tiled=True)
+    down_full = jnp.concatenate(lax.all_gather(down_weight, "sp"), axis=1)
     row_count, heads_here = log_decay.shape
     head_dim = queries.shape[1] // heads_here
     block_count = row_count // BLOCK

time: 645 us -> 603 us (0.935)
  waiting for transfers between devices: 502 us -> 445 us
  local copies, waits for them, and re-layouts: 28.1 us -> 43.2 us
    all_gather x1, waiting for transfers between devices: 183 us -> 141 us  [local(): down_full = jnp.concatenate(lax.all_gather(down_weight, 'sp'), axis=1)]
    reshape x1 -> x2, local copies, waits for them, and re-layouts: 0.01 us -> 15.1 us  [the longest x1 15.1 us: local(): down_full = jnp.concatenate(lax.all_gather(down_weight, 'sp'), axis=1)]
    all_gather x1, waiting for transfers between devices: 8.44 us -> 0.01 us  [local(): whole_rows = lax.all_gather(normed, 'tp', axis=0, tiled=True)]
    all_gather x1, waiting for transfers between devices: 145 us -> 139 us  [local(): lax.all_gather(gate_weight, 'sp', axis=0, tiled=True)]
  transfers between devices with their start and end apart: 7 -> 7, of which waited for: 7 -> 6; matrix products, arithmetic and copies ran while one was open for 2% -> 5% of each run, Pallas kernels for 0% -> 0%
where the time goes in v1:
time: 603 us; the launch traced here: 601 us
  waiting for transfers between devices  445 us (74%)
  local copies, waits for them, and re-layouts  43.2 us (7%)
  blocking collectives  42.5 us (7%)
  matrix products  31.5 us (5%)
  other arithmetic  24.6 us (4%)
  between operations  13.7 us (2%)
    all_gather x1, waiting for transfers between devices, local(): down_full = jnp.concatenate(lax.all_gather(down_weight, 'sp'), axis=1)  141 us
    all_gather x1, waiting for transfers between devices, local(): lax.all_gather(gate_weight, 'sp', axis=0, tiled=True)  139 us
    all_gather x1, waiting for transfers between devices, local(): lax.all_gather(up_weight, 'sp', axis=0, tiled=True)  133 us
    all_gather x1, blocking collectives, carried_in(): lax.all_gather(part.astype(kind), axis)  42.5 us
    all_gather x1, waiting for transfers between devices, carried_in(): lax.all_gather(part.astype(kind), axis)  17.2 us
    select_n x16, other arithmetic, turn(): return jax.tree.map(lambda a, b: jnp.where(reached, a, b), new, before)  16.2 us
    dot_general x1, matrix products, local(): down_terms = jnp.dot(hidden, down_full, preferred_element_type=jnp.float32)  15.9 us
    dynamic_update_slice x2, local copies, waits for them, and re-layouts, local(): final_state, within = lax.scan(block_pass, start_state, block_inputs)  15.3 us
  transfers between devices with their start and end apart: 7, of which 6 were waited for; matrix products, arithmetic and copies ran while one was open for 5% of the time, Pallas kernels for 0%

profile of v1, /device:TPU:0, one launch (start us, length us, event | category | flops | bytes accessed | tf_op | source)
XLA Modules:
  0.0 601.1 jit_solution(17356322570436744122)
XLA Ops:
  6.5 1.9 reshape.111
  8.4 1.7 reshape.112
  10.1 1.7 reshape.113
  12.7 24.1 %while.27 = (s32[]{:T(128)}, f32[4,128,128]{2,1,0:T(8,128)S(1)}, f32[2,128,4,128]{1,0,3,2:T(2,128)}, f32[2,128,4]{2,1,0:T(8,128)S(1)}, bf16[2,128,4,128]{3,2,1,0...) while((s32[]{:T(128)}, f32[4,128,128]{2,1,0:T(8,128)S(1)}, ...), condition=%wide.region_2.3_spmd.clone, body=%wide.region_0.2_spmd.clone.sunk | while | flops 319767040 | bytes 4260068 | solution.py:98
  16.5 7.7 %dynamic_update_slice.6 = f32[2,128,4,128]{1,0,3,2:T(2,128)} dynamic-update-slice(f32[2,128,4,128]{1,0,3,2:T(2,128)} %get-tuple-element.371, f32[1,128,4,128]{1,0,3,2:T(1,128)S(1)} %bitcast.119, s32[]{:T(128)} %get-tuple-element.369, s32[]{:T(128)} %constant.67.clone.1..sunk, s32[]{:T(128)} %constant.67.clone.1..sunk, s32[]{:T(128)} %constant.67.clone.1..sunk) | dynamic-update-slice | bytes 524292 | tf_op jit(solution)/shard_map/while/body/jit(dynamic_update_index_in_dim)/dynamic_update_slice | solution.py:98
  24.7 1.1 constant_dynamic-slice_fusion.6
  28.5 7.7 %dynamic_update_slice.6 = f32[2,128,4,128]{1,0,3,2:T(2,128)} dynamic-update-slice(f32[2,128,4,128]{1,0,3,2:T(2,128)} %get-tuple-element.371, f32[1,128,4,128]{1,0,3,2:T(1,128)S(1)} %bitcast.119, s32[]{:T(128)} %get-tuple-element.369, s32[]{:T(128)} %constant.67.clone.1..sunk, s32[]{:T(128)} %constant.67.clone.1..sunk, s32[]{:T(128)} %constant.67.clone.1..sunk) | dynamic-update-slice | bytes 524292 | tf_op jit(solution)/shard_map/while/body/jit(dynamic_update_index_in_dim)/dynamic_update_slice | solution.py:98
  37.6 1.2 reduce-window.6
  39.4 42.5 %all-gather.2 = bf16[16,1,4]{2,1,0:T(2,128)(2,1)S(1)} all-gather(bf16[1,1,4]{2,1,0:T(2,128)(2,1)S(1)} %bitcast.130), channel_id=1, replica_groups=mesh['sp'=16,'tp'=2] {'sp'}, dimensions={0}, use_global_device_ids=true | all-gather | bytes 136 | tf_op jit(solution)/shard_map/all_gather | solution.py:14
  82.0 1.5 reshape.114
  83.5 17.2 %all-gather.15.cloned.1.call-done = bf16[64,128,128]{2,1,0:T(8,128)(2,1)} async-done(((bf16[4,128,128]{2,1,0:T(8,128)(2,1)}), bf16[64,128,128]{2,1,0:T(8,128)(2,1)}) %all-gather.15.cloned.1.call-update) | async-done | bytes 2097168 | tf_op jit(solution)/shard_map/all_gather | solution.py:14
  100.7 16.8 %while.28 = (s32[]{:T(128)}, f32[4,128,128]{2,1,0:T(8,128)S(1)}, s32[]{:T(128)}, bf16[16,4]{1,0:T(8,128)(2,1)S(1)}, bf16[16,4,128,128]{3,2,1,0:T(8,128)(2,1)}, /*index=5*/s32[]{:T(128)}, s32[]{:T(128)}) while((s32[]{:T(128)}, f32[4,128,128]{2,1,0:T(8,128)S(1)}, s32[]{:T(128)}, bf16[16,4]{1,0:T(8,128)(2,1)S(1)}, ...), condition=%wide.region_6.7_spmd.clone, body=%wide.region_5.6_spmd.clone.sunk | while | flops 327688 | bytes 655505 | solution.py:31
  118.8 1.7 convolution_convert_fusion.1
  121.4 6.5 %reduce-scatter.3.cloned.1.call-done = bf16[128,2048]{1,0:T(8,128)(2,1)} async-done(((bf16[256,2048]{1,0:T(8,128)(2,1)}), bf16[128,2048]{1,0:T(8,128)(2,1)}) %reduce-scatter.3.cloned.1.call-update) | async-done | bytes 524304 | tf_op jit(solution)/shard_map/reduce_scatter | solution.py:125
  128.0 1.3 multiply_reduce_fusion
  129.3 2.0 multiply_convert_fusion
  132.7 140.7 %all-gather.17.cloned.1.call-done = bf16[45056,128]{1,0:T(8,128)(2,1)} async-done(((bf16[2816,128]{1,0:T(8,128)(2,1)}), bf16[45056,128]{1,0:T(8,128)(2,1)}) %all-gather.17.cloned.1.call-update) | async-done | bytes 11534352 | tf_op jit(solution)/shard_map/all_gather | solution.py:86
  273.4 15.1 %copy.133 = bf16[2816,16,128]{0,2,1:T(8,128)(2,1)} copy(bf16[2816,16,128]{2,0,1:T(8,128)(2,1)} %bitcast.121) | data formatting | bytes 23068672 | tf_op jit(solution)/shard_map/reshape | solution.py:86
  288.5 138.7 %all-gather.11.cloned.1.call-done = bf16[2048,2816]{1,0:T(8,128)(2,1)} async-done(((bf16[128,2816]{1,0:T(8,128)(2,1)}), bf16[2048,2816]{1,0:T(8,128)(2,1)}) %all-gather.11.cloned.1.call-update) | async-done | bytes 11534352 | tf_op jit(solution)/shard_map/all_gather | solution.py:83
  427.3 9.4 %fusion.32 = f32[256,2816]{1,0:T(8,128)} fusion(bf16[256,2048]{1,0:T(8,128)(2,1)} %all-gather.9.cloned.1.call-done, bf16[2048,2816]{1,0:T(8,128)(2,1)} %all-gather.11.cloned.1.call-done), kind=kOutput, calls=%fused_computation.68 | convolution fusion | flops 2952790016 | bytes 15466496 | tf_op jit(solution)/shard_map/dot_general | solution.py:138
  436.6 132.9 %all-gather.13.cloned.1.call-done = bf16[2048,2816]{1,0:T(8,128)(2,1)} async-done(((bf16[128,2816]{1,0:T(8,128)(2,1)}), bf16[2048,2816]{1,0:T(8,128)(2,1)}) %all-gather.13.cloned.1.call-update) | async-done | bytes 11534352 | tf_op jit(solution)/shard_map/all_gather | solution.py:84
  569.5 15.9 %convolution_convert_fusion = bf16[256,2048]{1,0:T(8,128)(2,1)} fusion(bf16[2816,2048]{0,1:T(8,128)(2,1)} %bitcast.122, bf16[256,2048]{1,0:T(8,128)(2,1)} %all-gather.9.cloned.1.call-done, bf16[2048,2816]{1,0:T(8,128)(2,1)} %all-gather.13.cloned.1.call-done, f32[256,2816]{1,0:T(8,128)} %fusion.32), kind=kOutput, calls=%fused_computation.32 | convolution fusion | flops 5910429696 | bytes 28049408 | tf_op jit(solution)/shard_map/dot_general | solution.py:141
  585.5 6.7 %reduce-scatter.5.cloned.1.call-done = bf16[128,2048]{1,0:T(8,128)(2,1)} async-done(((bf16[256,2048]{1,0:T(8,128)(2,1)}), bf16[128,2048]{1,0:T(8,128)(2,1)}) %reduce-scatter.5.cloned.1.call-update) | async-done | bytes 524304 | tf_op jit(solution)/shard_map/reduce_scatter | solution.py:142
  592.2 2.1 add_convert_fusion
  (120 shorter events, 29.7 us)
Async XLA Ops:
  6.5 112.3 %copy-start = (bf16[512,2048]{1,0:T(8,128)(2,1)S(1)}, bf16[512,2048]{1,0:T(8,128)(2,1)}, u32[]{:S(2)}) copy-start(bf16[512,2048]{1,0:T(8,128)(2,1)} %param.23) | copy-start | bytes 6291460
  6.5 94.2 %all-gather.15.cloned.1.call-start = ((), (), s32[]{:S(2)}) async-start(), calls=%async_computation.7 | async-start | bytes 2228224 | tf_op jit(solution)/shard_map/all_gather | solution.py:14
  12.7 24.9 %copy-start.5 = (f32[256,4]{0,1:T(4,128)S(1)}, f32[256,4]{0,1:T(4,128)}, u32[]{:S(2)}) copy-start(f32[256,4]{0,1:T(4,128)} %param.21) | copy-start | bytes 12292
  12.7 70.8 %copy-start.7 = (bf16[512]{0:T(512)(128)(2,1)S(1)}, bf16[512]{0:T(512)(128)(2,1)}, u32[]{:S(2)}) copy-start(bf16[512]{0:T(512)(128)(2,1)} %param.22) | copy-start | bytes 3076
  36.8 80.8 %copy-start.4 = (bf16[256,512]{1,0:T(8,128)(2,1)S(1)}, bf16[256,512]{1,0:T(8,128)(2,1)}, u32[]{:S(2)}) copy-start(bf16[256,512]{1,0:T(8,128)(2,1)} %param.17) | copy-start | bytes 786436
  37.5 90.5 %reduce-scatter.3.cloned.1.call-start = ((), (), s32[]{:S(2)}) async-start(), calls=%async_computation.2 | async-start | bytes 1572864 | tf_op jit(solution)/shard_map/reduce_scatter | solution.py:125
  117.5 1.3 copy-start.8
  118.8 2.6 copy-start.6
  118.8 9.1 %copy-start.2 = (bf16[128,2048]{1,0:T(8,128)(2,1)S(1)}, bf16[128,2048]{1,0:T(8,128)(2,1)}, u32[]{:S(2)}) copy-start(bf16[128,2048]{1,0:T(8,128)(2,1)} %param.16) | copy-start | bytes 1572868
  120.6 152.8 %all-gather.17.cloned.1.call-start = ((), (), s32[]{:S(2)}) async-start(), calls=%async_computation.8 | async-start | bytes 12255232 | tf_op jit(solution)/shard_map/all_gather | solution.py:86
  121.3 167.2 %all-gather.9.cloned.1.call-start = ((), (), s32[]{:S(2)}) async-start(), calls=%async_computation.3 | async-start | bytes 1572864 | tf_op jit(solution)/shard_map/all_gather | solution.py:137
  131.3 295.9 %all-gather.11.cloned.1.call-start = ((), (), s32[]{:S(2)}) async-start(), calls=%async_computation.4 | async-start | bytes 12255232 | tf_op jit(solution)/shard_map/all_gather | solution.py:83
  131.9 437.6 %all-gather.13.cloned.1.call-start = ((), (), s32[]{:S(2)}) async-start(), calls=%async_computation.5 | async-start | bytes 12255232 | tf_op jit(solution)/shard_map/all_gather | solution.py:84
  132.5 459.7 %reduce-scatter.5.cloned.1.call-start = ((), (), s32[]{:S(2)}) async-start(), calls=%async_computation.6 | async-start | bytes 1572864 | tf_op jit(solution)/shard_map/reduce_scatter | solution.py:142
  569.5 22.7 %copy-start.3 = (bf16[128,2048]{1,0:T(8,128)(2,1)S(1)}, bf16[128,2048]{1,0:T(8,128)(2,1)}, u32[]{:S(2)}) copy-start(bf16[128,2048]{1,0:T(8,128)(2,1)} %reduce-scatter.3.cloned.1.call-done) | copy-start | bytes 1572868
  569.5 24.8 %copy-start.1 = (bf16[512,2048]{1,0:T(8,128)(2,1)S(1)}, bf16[512,2048]{1,0:T(8,128)(2,1)}, u32[]{:S(2)}) copy-start(bf16[512,2048]{1,0:T(8,128)(2,1)} %param.23) | copy-start | bytes 6291460
Sparse Core Ops, SparseCore 0:
  37.6 63.0 all-gather.14
  120.7 7.1 reduce-scatter.2
  130.7 142.6 all-gather.16
  274.8 7.1 all-gather.8
  284.6 142.5 all-gather.10
  429.9 139.5 all-gather.12
  585.6 6.5 reduce-scatter.4
